TPU v7x, 512 devices: a whole 4x4x16 slice. The times are simulated.
512 devices in a mesh: sp: 64 (over z, y), tp: 8 (over x, core).
Axes of the slice: x: 4, y: 4, z: 16, core: 2. Of those that a mesh axis runs over, the one named last changes fastest.
Arguments:
- tokens: bfloat16 [49152, 2048], P(('sp', 'tp')), may hold values from -6 to 6
- input_gain: float32 [2048], replicated, may hold values from 0.1 to 1.9
- branch_value: bfloat16 [2048, 1024], P('sp', 'tp'), may hold values from -0.125 to 0.125
- branch_gate: bfloat16 [2048, 1024], P('sp', 'tp'), may hold values from -0.125 to 0.125
- query_weight: bfloat16 [2048, 1024], P('sp', 'tp'), may hold values from -0.125 to 0.125
- key_weight: bfloat16 [2048, 1024], P('sp', 'tp'), may hold values from -0.125 to 0.125
- value_weight: bfloat16 [2048, 1024], P('sp', 'tp'), may hold values from -0.125 to 0.125
- swish_weight: bfloat16 [2048, 1024], P('sp', 'tp'), may hold values from -0.125 to 0.125
- kernel_taps: float32 [31, 1024], P(None, 'tp'), may hold values from -8 to 8
- channel_gain: float32 [1024], P('tp'), may hold values from 0.1 to 1.9
- decay_logs: float32 [16, 49152], P('tp', 'sp'), may hold values from -1.5 to 0
- start_state: float32 [2, 16, 64, 64], P(None, 'tp')
- head_gain: float32 [1024], P('tp'), may hold values from 0.1 to 1.9
- output_conv: bfloat16 [1024, 2048], P('tp', 'sp'), may hold values from -0.125 to 0.125
- output_heads: bfloat16 [1024, 2048], P('tp', 'sp'), may hold values from -0.125 to 0.125
Outputs:
- mixed: bfloat16 [49152, 2048], P(('sp', 'tp'))
All inputs are finite; a program needn't handle non-finite values.
Results may differ from a plain program's by a relative error of at most 0.018.
Values may be sent and summed in bfloat16 or wider, within the bound.
No kernel may reach another device: no remote copies, remote signals or barrier semaphores. Data moves between devices by JAX's collectives and lax.ppermute only.
A program may use at most 64 MiB of HBM per device.

v0:
```python
import jax
import jax.numpy as jnp
from jax import lax
from jax.sharding import Mesh
from jax.sharding import PartitionSpec as P

DC = 1024
HD = 64
BLOCK = 256
SP = ("sp_0", "sp_1")
SP_TP = ("sp_0", "sp_1", "tp")
EPSILON = 1e-06


def sent_together(arrays, axis, dim, along):
    ends, at = ([], 0)
    for a in arrays[:-1]:
        at += a.shape[along]
        ends.append(at)
    both = jnp.concatenate(arrays, axis=along)
    return tuple(jnp.split(lax.all_gather(both, axis, axis=dim, tiled=True), ends, axis=along))


def with_halo(x, sides, width):
    for axis, dim in sides:
        count, length = (lax.axis_size(axis), x.shape[dim])
        up = [(i, (i + 1) % count) for i in range(count - 1)]
        down = [(j, i) for i, j in up]
        last = lax.slice_in_dim(x, length - width, length, axis=dim)
        first = lax.slice_in_dim(x, 0, width, axis=dim)
        before = lax.ppermute(last, axis, up)
        after = lax.ppermute(first, axis, down)
        x = jnp.concatenate([before, x, after], axis=dim)
    return x


def copy_for_each(x, axis):
    count = lax.axis_size(axis)
    return lax.all_to_all(jnp.broadcast_to(x[None], (count, *x.shape)), axis, 0, 0, tiled=True)


def over_copies(x, axis):
    everything = copy_for_each(x, axis)
    return jnp.sum(everything, axis=0)


def together(arrays, axis):
    ends = [0]
    for a in arrays:
        ends.append(ends[-1] + a.size)
    subtotal = over_copies(jnp.concatenate([a.ravel() for a in arrays]), axis)
    return tuple((subtotal[b:e].reshape(a.shape) for a, b, e in zip(arrays, ends, ends[1:])))


def filled_with(x, identity):
    return jax.tree.map(
        lambda part, zero: jnp.zeros_like(part) + jnp.asarray(zero, part.dtype), x, identity
    )


def all_in_one(x, axis):
    leaves = jax.tree.leaves(x)
    order = sorted(range(len(leaves)), key=lambda k: -leaves[k].size)
    width = (1, *leaves[order[0]].shape)[-1]
    lines = [
        jnp.pad(leaves[k].reshape(-1), (0, -leaves[k].size % width)).reshape(-1, width)
        for k in order
    ]
    both, at, found = (lax.all_gather(jnp.concatenate(lines), axis), 0, {})
    for k, line in zip(order, lines):
        section = both[:, at : at + len(line)].reshape(len(both), -1)
        found[k] = section[:, : leaves[k].size].reshape(-1, *leaves[k].shape)
        at += len(line)
    numbers = iter(range(len(leaves)))
    return jax.tree.map(lambda _: found[next(numbers)], x)


def prefix_by_axis(x, axes, combine, identity, reverse):
    before = start = filled_with(x, identity)
    subtotal = x
    for axis in reversed(axes):
        count, position = (lax.axis_size(axis), lax.axis_index(axis))
        pieces = all_in_one(
            jax.tree.map(
                lambda part, kind: part.astype(kind), subtotal, (jnp.bfloat16, jnp.bfloat16)
            ),
            axis,
        )
        inside, subtotal = (start, start)
        for k in reversed(range(count)) if reverse else range(count):
            passed = k > position if reverse else k < position
            subtotal = combine(
                subtotal, jax.tree.map(lambda part, own: part[k].astype(own.dtype), pieces, x)
            )
            inside = jax.tree.map(lambda new, old: jnp.where(passed, new, old), subtotal, inside)
        before = combine(inside, before)
    return before


def rows_first(arrays, axis, dims):
    turned = [jnp.moveaxis(a, dim, 0) for a, dim in zip(arrays, dims)]
    both = jnp.concatenate([t.reshape(len(t), -1) for t in turned], axis=1)
    out, at, gathered = (lax.all_gather(both, axis, axis=0, tiled=True), 0, [])
    for t, dim in zip(turned, dims):
        section = out[:, at : at + t[0].size].reshape(-1, *t.shape[1:])
        gathered.append(jnp.moveaxis(section, 0, dim))
        at += t[0].size
    return tuple(gathered)


def split_up(x, dim, count):
    shape = x.shape
    pieces = x.reshape(*shape[:dim], count, shape[dim] // count, *shape[dim + 1 :])
    return jnp.moveaxis(pieces, dim, 0)


def sum_at_owner(x, axis, dim):
    pieces = split_up(x, dim, lax.axis_size(axis))
    arrived = lax.all_to_all(pieces, axis, split_axis=0, concat_axis=0, tiled=True)
    return arrived.astype(jnp.float32).sum(axis=0)


def block_states(scaled_keys, values_block, running):
    closing = running[:, :, -1:]
    totals = jnp.exp(closing[:, :, 0])
    toward_end = jnp.exp(closing - running).transpose(0, 2, 1)[:, :, :, None]
    from_start = jnp.exp(running).transpose(0, 2, 1)[:, :, :, None]
    forward = jnp.einsum("nshd,nshe->nhde", scaled_keys * toward_end, values_block)
    backward = jnp.einsum("nshd,nshe->nhde", scaled_keys * from_start, values_block)
    return (totals, forward, backward)


def block_outputs(queries, scaled_keys, values_block, running, forward_in, backward_in):
    length = queries.shape[1]
    scores = jnp.einsum("nthd,nshd->nhts", queries, scaled_keys)
    distance = jnp.abs(running[:, :, :, None] - running[:, :, None, :])
    weights = jnp.exp(-distance) + jnp.eye(length, dtype=jnp.float32)
    within = jnp.einsum("nhts,nshe->nthe", scores * weights, values_block)
    from_start = jnp.exp(running).transpose(0, 2, 1)[:, :, :, None]
    toward_end = jnp.exp(running[:, :, -1:] - running).transpose(0, 2, 1)[:, :, :, None]
    earlier = jnp.einsum("nthd,nhde->nthe", queries, forward_in)
    after_part = jnp.einsum("nthd,nhde->nthe", queries, backward_in)
    return within + from_start * earlier + toward_end * after_part


def head_output(retained, gates_in, head_gain):
    row_count = retained.shape[0]
    centred = retained - jnp.mean(retained, axis=2, keepdims=True)
    scaled = centred * lax.rsqrt(jnp.mean(centred * centred, axis=2, keepdims=True) + EPSILON)
    flattened = scaled.reshape(row_count, -1) * head_gain[None, :]
    return (flattened * jax.nn.silu(gates_in.astype(jnp.float32))).astype(jnp.bfloat16)


def normalize(token_block, input_gain):
    widened = token_block.astype(jnp.float32)
    inverse = lax.rsqrt(jnp.mean(widened * widened, axis=1, keepdims=True) + EPSILON)
    return (widened * inverse * input_gain[None, :]).astype(jnp.bfloat16)


def input_mix(products):
    gated_rows = (products[0] * jax.nn.sigmoid(products[1])).astype(jnp.bfloat16)
    others = [member.astype(jnp.bfloat16) for member in products[2:]]
    return jnp.concatenate([gated_rows] + others, axis=1)


def combine_branches(earlier, latter):
    return (earlier[0] * latter[0], latter[0][:, None, None] * earlier[1] + latter[1])


def body(
    tokens,
    input_gain,
    branch_value,
    branch_gate,
    query_weight,
    key_weight,
    value_weight,
    swish_weight,
    kernel_taps,
    channel_gain,
    decay_logs,
    start_state,
    head_gain,
    output_conv,
    output_heads,
):
    projections = (branch_value, branch_gate, query_weight, key_weight, value_weight, swish_weight)
    full_column_count = sent_together(
        (
            projections[0],
            projections[1],
            projections[2],
            projections[3],
            projections[4],
            projections[5],
        ),
        SP,
        0,
        1,
    )
    normed = normalize(lax.all_gather(tokens, "tp", axis=0, tiled=True), input_gain)
    packed = input_mix(
        tuple(
            (
                jnp.dot(normed, weight, preferred_element_type=jnp.float32)
                for weight in full_column_count
            )
        )
    )
    value_width = branch_value.shape[1]
    head_width = query_weight.shape[1]
    row_count = packed.shape[0]
    gated_rows = packed[:, :value_width]
    queries_in = packed[:, value_width : value_width + head_width]
    keys_in = packed[:, value_width + head_width : value_width + 2 * head_width]
    values_in = packed[:, value_width + 2 * head_width : value_width + 3 * head_width]
    gates_in = packed[:, value_width + 3 * head_width :]
    half_width = kernel_taps.shape[0] // 2
    padded = with_halo(gated_rows, ((SP, 0),), half_width).astype(jnp.float32)
    convolved = jnp.zeros((row_count, value_width), jnp.float32)
    for offset in range(kernel_taps.shape[0]):
        convolved = convolved + kernel_taps[offset][None, :] * padded[offset : offset + row_count]
    moments = together((jnp.sum(convolved, axis=1), jnp.sum(convolved * convolved, axis=1)), "tp")
    average = (moments[0] / DC)[:, None]
    squares = (moments[1] / DC)[:, None]
    normalized = (convolved - average) * lax.rsqrt(squares - average * average + EPSILON)
    branch_out = jax.nn.silu(normalized * channel_gain[None, :]).astype(jnp.bfloat16)
    local_heads = head_width // HD
    blocks = row_count // BLOCK

    def split_heads(matrix):
        return matrix.astype(jnp.float32).reshape(blocks, BLOCK, local_heads, HD)

    query_blocks = split_heads(queries_in)
    key_blocks = split_heads(keys_in) * HD ** (-0.5)
    value_blocks = split_heads(values_in)
    running = jnp.cumsum(decay_logs.reshape(local_heads, blocks, BLOCK).transpose(1, 0, 2), axis=2)
    totals, forward, backward = block_states(key_blocks, value_blocks, running)
    forward_part = []
    forward_scale = []
    carried = jnp.zeros_like(forward[0])
    factor = jnp.ones_like(totals[0])
    for block_index in range(blocks):
        forward_part.append(carried)
        forward_scale.append(factor)
        carried = totals[block_index][:, None, None] * carried + forward[block_index]
        factor = factor * totals[block_index]
    device_forward = carried
    device_total = factor
    backward_part = [None] * blocks
    reverse_direction_scale = [None] * blocks
    carried = jnp.zeros_like(backward[0])
    factor = jnp.ones_like(totals[0])
    for block_index in reversed(range(blocks)):
        backward_part[block_index] = carried
        reverse_direction_scale[block_index] = factor
        carried = totals[block_index][:, None, None] * carried + backward[block_index]
        factor = factor * totals[block_index]
    identity = (jnp.ones_like(device_total), jnp.zeros_like(device_forward))
    before = prefix_by_axis((device_total, device_forward), SP, combine_branches, identity, False)
    after = prefix_by_axis((device_total, carried), SP, combine_branches, identity, True)
    enter_forward = before[1] + before[0][:, None, None] * start_state[0]
    enter_backward = after[1] + after[0][:, None, None] * start_state[1]
    forward_in = jnp.stack(
        [
            forward_scale[block_index][:, None, None] * enter_forward + forward_part[block_index]
            for block_index in range(blocks)
        ]
    )
    backward_in = jnp.stack(
        [
            reverse_direction_scale[block_index][:, None, None] * enter_backward
            + backward_part[block_index]
            for block_index in range(blocks)
        ]
    )
    retained = block_outputs(
        query_blocks, key_blocks, value_blocks, running, forward_in, backward_in
    )
    heads_out = head_output(retained.reshape(row_count, local_heads, HD), gates_in, head_gain)
    out_columns = rows_first((output_conv, output_heads), SP, (1, 1))
    combined = jnp.dot(branch_out, out_columns[0], preferred_element_type=jnp.float32)
    summed = sum_at_owner(
        (combined + jnp.dot(heads_out, out_columns[1], preferred_element_type=jnp.float32)).astype(
            jnp.bfloat16
        ),
        "tp",
        0,
    )
    return summed.astype(jnp.bfloat16)


def solution(mesh):
    split = Mesh(mesh.devices.reshape(16, 4, mesh.shape["tp"]), ("sp_0", "sp_1", "tp"))
    in_specs = (
        P(SP_TP, None),
        P(),
        P(SP, "tp"),
        P(SP, "tp"),
        P(SP, "tp"),
        P(SP, "tp"),
        P(SP, "tp"),
        P(SP, "tp"),
        P(None, "tp"),
        P("tp"),
        P("tp", SP),
        P(None, "tp", None, None),
        P("tp"),
        P("tp", SP),
        P("tp", SP),
    )
    out_specs = P(SP_TP, None)
    return jax.shard_map(body, mesh=split, in_specs=in_specs, out_specs=out_specs, check_vma=False)
```

profile of v0, /device:TPU:32, one launch (start us, length us, event | category | flops | bytes accessed | tf_op | source)
XLA Modules:
  0.0 487.4 jit_solution(7230470878673933972)
XLA Ops:
  14.4 1.8 reduce-window.6
  17.3 1.6 slice_bitcast_fusion.61
  18.9 1.6 slice_bitcast_fusion.62
  27.8 21.2 %all-gather.12.cloned.1.call-done = bf16[768,2048]{1,0:T(8,128)(2,1)} async-done(((bf16[96,2048]{1,0:T(8,128)(2,1)}), bf16[768,2048]{1,0:T(8,128)(2,1)}) %all-gather.12.cloned.1.call-update) | async-done | bytes 3145744 | tf_op jit(solution)/shard_map/all_gather | solution.py:201
  48.9 2.7 fusion
  52.6 143.0 %all-gather.14.cloned.1.call-done = bf16[2048,768]{1,0:T(8,128)(2,1)} async-done(((bf16[32,768]{1,0:T(8,128)(2,1)}), bf16[2048,768]{1,0:T(8,128)(2,1)}) %all-gather.14.cloned.1.call-update) | async-done | bytes 3145744 | tf_op jit(solution)/shard_map/all_gather | solution.py:21
  195.6 2.0 convolution_convert_fusion.3
  199.8 2.8 fusion.29
  202.7 1.9 copy.305
  204.6 2.0 reshape.1739
  206.6 2.0 broadcast_multiply_fusion.2
  210.5 1.5 copy.317
  212.1 1.5 copy.319
  213.6 1.5 copy.318
  215.8 1.5 copy.348
  217.3 1.5 copy.350
  218.9 1.5 copy.349
  222.0 12.1 %all-gather.4 = bf16[4,129,64]{1,2,0:T(8,128)(2,1)S(1)} all-gather(bf16[1,129,64]{1,2,0:T(8,128)(2,1)S(1)} %get-tuple-element.78), channel_id=2, replica_groups=mesh['sp_0'=16,'sp_1'=4,'tp'=8] {'sp_1'}, dimensions={0}, use_global_device_ids=true | all-gather | bytes 82560 | tf_op jit(solution)/shard_map/all_gather | solution.py:69
  236.0 12.0 %all-gather.6 = bf16[4,129,64]{1,2,0:T(8,128)(2,1)S(1)} all-gather(bf16[1,129,64]{1,2,0:T(8,128)(2,1)S(1)} %get-tuple-element.79), channel_id=4, replica_groups=mesh['sp_0'=16,'sp_1'=4,'tp'=8] {'sp_1'}, dimensions={0}, use_global_device_ids=true | all-gather | bytes 82560 | tf_op jit(solution)/shard_map/all_gather | solution.py:69
  250.7 1.3 mul.1869
  252.0 1.3 mul.1871
  259.6 1.3 mul.1879
  263.7 29.0 %all-gather.7 = bf16[16,129,64]{1,2,0:T(8,128)(2,1)S(1)} all-gather(bf16[1,129,64]{1,2,0:T(8,128)(2,1)S(1)} %maximum_bitcast_fusion.1), channel_id=5, replica_groups=mesh['sp_0'=16,'sp_1'=4,'tp'=8] {'sp_0'}, dimensions={0}, use_global_device_ids=true | all-gather | bytes 280704 | tf_op jit(solution)/shard_map/all_gather | solution.py:69
  297.8 1.3 mul.1768
  303.0 1.3 mul.1774
  310.8 31.0 %all-gather.5 = bf16[16,129,64]{1,2,0:T(8,128)(2,1)S(1)} all-gather(bf16[1,129,64]{1,2,0:T(8,128)(2,1)S(1)} %maximum_bitcast_fusion), channel_id=3, replica_groups=mesh['sp_0'=16,'sp_1'=4,'tp'=8] {'sp_0'}, dimensions={0}, use_global_device_ids=true | all-gather | bytes 280704 | tf_op jit(solution)/shard_map/all_gather | solution.py:69
  345.6 2.7 convolution_convert_fusion.2
  348.3 1.9 reshape.1847
  350.2 1.9 copy.306
  352.1 1.5 copy.339
  353.5 1.5 copy.341
  355.0 1.5 copy.340
  356.5 1.5 copy.342
  358.0 1.5 copy.370
  359.4 1.5 copy.372
  360.9 1.5 copy.371
  362.4 1.5 copy.373
  363.9 2.0 fusion.41
  365.9 2.0 fusion.27
  368.8 1.9 collective-permute-start
  370.7 6.2 %collective-permute-start.1 = (bf16[15,128]{1,0:T(8,128)(2,1)}, bf16[15,128]{1,0:T(8,128)(2,1)}, u32[]{:S(2)}, u32[]{:S(2)}) collective-permute-start(bf16[15,128]{1,0:T(8,128)(2,1)} %get-tuple-element.69), channel_id=1, source_target_pairs={{8,0},{16,8},{24,16},{32,24},{40,32},{48,40},{56,48},{64,56},{72,6... | collective-permute-start | bytes 11528 | tf_op jit(solution)/shard_map/ppermute | solution.py:32
  411.4 1.5 fusion.160
  413.6 4.3 all-to-all-start
  420.8 2.6 all-to-all-done
  423.5 4.7 fusion.38
  428.2 7.7 %add_convert_fusion = bf16[768,2048]{1,0:T(8,128)(2,1)S(1)} fusion(f32[768,2048]{1,0:T(8,128)} %fusion.38, bf16[2048,256]{1,0:T(8,128)(2,1)} %all-gather.16.cloned.1.call-done, bf16[768,2048]{1,0:T(8,128)(2,1)} %copy-done.1, bf16[2048,768]{1,0:T(8,128)(2,1)} %all-gather.14.cloned.1.call-done, f32[768,128]{1,0:T(8,128)S(1)} %copy.379, ...), kind=kOutput, calls=%fused_computation.5 | convolution fusion | flops 809533440 | bytes 14811648 | tf_op jit(solution)/shard_map/dot_general | solution.py:284
  435.9 41.7 %all_to_all.11 = bf16[8,96,2048]{2,1,0:T(8,128)(2,1)} all-to-all(bf16[8,96,2048]{2,1,0:T(8,128)(2,1)S(1)} %bitcast.522), channel_id=1, replica_groups=mesh['sp_0'=16,'sp_1'=4,'tp'=8] {'tp'}, dimensions={0} | all-to-all | bytes 6291456 | tf_op jit(solution)/shard_map/all_to_all | solution.py:119
  477.6 3.3 reduce_sum.72
  (303 shorter events, 93.9 us)
Async XLA Ops:
  6.5 45.1 %copy-start.26 = (f32[2048]{0:T(1024)S(1)}, f32[2048]{0:T(1024)}, u32[]{:S(2)}) copy-start(f32[2048]{0:T(1024)} %param.16) | copy-start | bytes 24580
  6.5 42.4 %all-gather.12.cloned.1.call-start = ((), (), s32[]{:S(2)}) async-start(), calls=%async_computation.2 | async-start | bytes 3538944 | tf_op jit(solution)/shard_map/all_gather | solution.py:201
  7.3 188.3 %all-gather.14.cloned.1.call-start = ((), (), s32[]{:S(2)}) async-start(), calls=%async_computation.3 | async-start | bytes 3194880 | tf_op jit(solution)/shard_map/all_gather | solution.py:21
  12.2 411.3 %all-gather.16.cloned.1.call-start = ((), (), s32[]{:S(2)}) async-start(), calls=%async_computation.4 | async-start | bytes 1064960 | tf_op jit(solution)/shard_map/all_gather | solution.py:103
  21.6 30.0 %copy-start.27 = (f32[2]{0:T(128)}, f32[2]{0:T(128)S(1)}, u32[]{:S(2)}) copy-start(f32[2]{0:T(128)S(1)} %get-tuple-element.9) | copy-start | bytes 28
  21.6 30.9 %copy-start.32 = (f32[2]{0:T(128)}, f32[2]{0:T(128)S(1)}, u32[]{:S(2)}) copy-start(f32[2]{0:T(128)S(1)} %get-tuple-element.8) | copy-start | bytes 28
  23.6 29.0 %copy-start.28 = (f32[2]{0:T(128)}, f32[2]{0:T(128)S(1)}, u32[]{:S(2)}) copy-start(f32[2]{0:T(128)S(1)} %get-tuple-element.155) | copy-start | bytes 28
  23.6 29.0 %copy-start.30 = (f32[2]{0:T(128)}, f32[2]{0:T(128)S(1)}, u32[]{:S(2)}) copy-start(f32[2]{0:T(128)S(1)} %get-tuple-element.156) | copy-start | bytes 28
  52.6 313.3 %copy-start.1 = (bf16[768,2048]{1,0:T(8,128)(2,1)}, bf16[768,2048]{1,0:T(8,128)(2,1)S(1)}, u32[]{:S(2)}) copy-start(bf16[768,2048]{1,0:T(8,128)(2,1)S(1)} %fusion.2) | copy-start | bytes 9437188
  199.8 8.8 %copy-start.2 = (bf16[3,256,2,64]{1,3,2,0:T(8,128)(2,1)}, bf16[3,256,2,64]{1,3,2,0:T(8,128)(2,1)S(1)}, u32[]{:S(2)}) copy-start(bf16[3,256,2,64]{1,3,2,0:T(8,128)(2,1)S(1)} %copy.311) | copy-start | bytes 589828
  199.8 6.8 %copy-start.25 = (f32[3,256,2]{1,0,2:T(4,128)S(1)}, f32[3,256,2]{1,0,2:T(4,128)}, u32[]{:S(2)}) copy-start(f32[3,256,2]{1,0,2:T(4,128)} %copy.345) | copy-start | bytes 18436
  234.2 59.2 %copy-start.21 = (bf16[4,64]{1,0:T(4,128)(2,1)}, bf16[4,64]{1,0:T(4,128)(2,1)S(1)}, u32[]{:S(2)}) copy-start(bf16[4,64]{1,0:T(4,128)(2,1)S(1)} %slice_reduce_fusion.1) | copy-start | bytes 1540
  248.1 94.4 %copy-start.23 = (bf16[4,64]{1,0:T(4,128)(2,1)}, bf16[4,64]{1,0:T(4,128)(2,1)S(1)}, u32[]{:S(2)}) copy-start(bf16[4,64]{1,0:T(4,128)(2,1)S(1)} %slice_reduce_fusion) | copy-start | bytes 1540
  368.0 9.0 %copy-start.17 = (bf16[768,128]{1,0:T(8,128)(2,1)}, bf16[768,128]{1,0:T(8,128)(2,1)S(1)}, u32[]{:S(2)}) copy-start(bf16[768,128]{1,0:T(8,128)(2,1)S(1)} %fusion.27) | copy-start | bytes 589828
  368.0 35.6 %copy-start.19 = (f32[1,128,64]{1,2,0:T(8,128)S(1)}, f32[1,128,64]{1,2,0:T(8,128)}, u32[]{:S(2)}) copy-start(f32[1,128,64]{1,2,0:T(8,128)} %get-tuple-element.45) | copy-start | bytes 98308
  368.0 35.7 %copy-start.24 = (bf16[4,64]{1,0:T(4,128)(2,1)S(1)}, bf16[4,64]{1,0:T(4,128)(2,1)}, u32[]{:S(2)}) copy-start(bf16[4,64]{1,0:T(4,128)(2,1)} %copy-done.23) | copy-start | bytes 1540
  368.0 35.7 %copy-start.43 = (f32[2]{0:T(128)S(1)}, f32[2]{0:T(128)}, u32[]{:S(2)}) copy-start(f32[2]{0:T(128)} %get-tuple-element.23) | copy-start | bytes 28
  368.0 35.8 %copy-start.22 = (bf16[4,64]{1,0:T(4,128)(2,1)S(1)}, bf16[4,64]{1,0:T(4,128)(2,1)}, u32[]{:S(2)}) copy-start(bf16[4,64]{1,0:T(4,128)(2,1)} %copy-done.21) | copy-start | bytes 1540
  368.0 35.8 %copy-start.42 = (f32[2]{0:T(128)S(1)}, f32[2]{0:T(128)}, u32[]{:S(2)}) copy-start(f32[2]{0:T(128)} %get-tuple-element.15) | copy-start | bytes 28
  368.0 35.8 %copy-start.11 = (f32[1,128,64]{2,1,0:T(8,128)S(1)}, f32[1,128,64]{2,1,0:T(8,128)}, u32[]{:S(2)}) copy-start(f32[1,128,64]{2,1,0:T(8,128)} %copy.339) | copy-start | bytes 98308
  368.0 35.8 %copy-start.12 = (f32[1,128,64]{2,1,0:T(8,128)S(1)}, f32[1,128,64]{2,1,0:T(8,128)}, u32[]{:S(2)}) copy-start(f32[1,128,64]{2,1,0:T(8,128)} %copy.341) | copy-start | bytes 98308
  368.0 35.8 %copy-start.13 = (f32[1,128,64]{2,1,0:T(8,128)S(1)}, f32[1,128,64]{2,1,0:T(8,128)}, u32[]{:S(2)}) copy-start(f32[1,128,64]{2,1,0:T(8,128)} %copy.340) | copy-start | bytes 98308
  368.0 35.8 %copy-start.14 = (f32[1,128,64]{2,1,0:T(8,128)S(1)}, f32[1,128,64]{2,1,0:T(8,128)}, u32[]{:S(2)}) copy-start(f32[1,128,64]{2,1,0:T(8,128)} %copy.342) | copy-start | bytes 98308
  368.1 35.8 %copy-start.29 = (f32[2]{0:T(128)S(1)}, f32[2]{0:T(128)}, u32[]{:S(2)}) copy-start(f32[2]{0:T(128)} %copy-done.28) | copy-start | bytes 28
  368.1 35.8 %copy-start.33 = (f32[2]{0:T(128)S(1)}, f32[2]{0:T(128)}, u32[]{:S(2)}) copy-start(f32[2]{0:T(128)} %copy-done.32) | copy-start | bytes 28
  368.1 35.8 %copy-start.35 = (f32[2]{0:T(128)S(1)}, f32[2]{0:T(128)}, u32[]{:S(2)}) copy-start(f32[2]{0:T(128)} %get-tuple-element.147) | copy-start | bytes 28
  368.1 35.8 %copy-start.36 = (f32[2]{0:T(128)S(1)}, f32[2]{0:T(128)}, u32[]{:S(2)}) copy-start(f32[2]{0:T(128)} %get-tuple-element.114) | copy-start | bytes 28
  368.1 35.8 %copy-start.37 = (f32[2]{0:T(128)S(1)}, f32[2]{0:T(128)}, u32[]{:S(2)}) copy-start(f32[2]{0:T(128)} %get-tuple-element.115) | copy-start | bytes 28
  368.1 35.8 %copy-start.38 = (f32[2]{0:T(128)S(1)}, f32[2]{0:T(128)}, u32[]{:S(2)}) copy-start(f32[2]{0:T(128)} %get-tuple-element.116) | copy-start | bytes 28
  368.1 35.8 %copy-start.39 = (f32[2]{0:T(128)S(1)}, f32[2]{0:T(128)}, u32[]{:S(2)}) copy-start(f32[2]{0:T(128)} %get-tuple-element.117) | copy-start | bytes 28
  368.1 35.8 %copy-start.40 = (f32[2]{0:T(128)S(1)}, f32[2]{0:T(128)}, u32[]{:S(2)}) copy-start(f32[2]{0:T(128)} %get-tuple-element.118) | copy-start | bytes 28
  368.1 37.0 %copy-start.7 = (f32[1,128,64]{2,1,0:T(8,128)S(1)}, f32[1,128,64]{2,1,0:T(8,128)}, u32[]{:S(2)}) copy-start(f32[1,128,64]{2,1,0:T(8,128)} %copy.370) | copy-start | bytes 98308
  368.1 37.0 %copy-start.8 = (f32[1,128,64]{2,1,0:T(8,128)S(1)}, f32[1,128,64]{2,1,0:T(8,128)}, u32[]{:S(2)}) copy-start(f32[1,128,64]{2,1,0:T(8,128)} %copy.372) | copy-start | bytes 98308
  368.2 37.0 %copy-start.9 = (f32[1,128,64]{2,1,0:T(8,128)S(1)}, f32[1,128,64]{2,1,0:T(8,128)}, u32[]{:S(2)}) copy-start(f32[1,128,64]{2,1,0:T(8,128)} %copy.371) | copy-start | bytes 98308
  368.2 37.0 %copy-start.10 = (f32[1,128,64]{2,1,0:T(8,128)S(1)}, f32[1,128,64]{2,1,0:T(8,128)}, u32[]{:S(2)}) copy-start(f32[1,128,64]{2,1,0:T(8,128)} %copy.373) | copy-start | bytes 98308
  368.8 41.5 %collective-permute-start = (bf16[15,128]{1,0:T(8,128)(2,1)}, bf16[15,128]{1,0:T(8,128)(2,1)}, u32[]{:S(2)}, u32[]{:S(2)}) collective-permute-start(bf16[15,128]{1,0:T(8,128)(2,1)} %get-tuple-element.68), channel_id=1, source_target_pairs={{0,8},{8,16},{16,24},{24,32},{32,40},{40,48},{48,56},{56,64},{64,7... | collective-permute-start | bytes 11528 | tf_op jit(solution)/shard_map/ppermute | solution.py:31
  370.7 39.6 %collective-permute-start.1 = (bf16[15,128]{1,0:T(8,128)(2,1)}, bf16[15,128]{1,0:T(8,128)(2,1)}, u32[]{:S(2)}, u32[]{:S(2)}) collective-permute-start(bf16[15,128]{1,0:T(8,128)(2,1)} %get-tuple-element.69), channel_id=1, source_target_pairs={{8,0},{16,8},{24,16},{32,24},{40,32},{48,40},{56,48},{64,56},{72,6... | collective-permute-start | bytes 11528 | tf_op jit(solution)/shard_map/ppermute | solution.py:32
  382.9 24.6 %copy-start.4 = (bf16[3,256,2,64]{1,3,2,0:T(8,128)(2,1)S(1)}, bf16[3,256,2,64]{1,3,2,0:T(8,128)(2,1)}, u32[]{:S(2)}) copy-start(bf16[3,256,2,64]{1,3,2,0:T(8,128)(2,1)} %copy.306) | copy-start | bytes 589828
  395.8 13.6 %copy-start.3 = (bf16[3,256,2,64]{1,3,2,0:T(8,128)(2,1)S(1)}, bf16[3,256,2,64]{1,3,2,0:T(8,128)(2,1)}, u32[]{:S(2)}) copy-start(bf16[3,256,2,64]{1,3,2,0:T(8,128)(2,1)} %copy-done.2) | copy-start | bytes 589828
  406.4 4.6 copy-start.44
  406.4 4.6 copy-start.45
  406.4 4.6 copy-start.46
  406.4 4.6 copy-start.47
  406.4 4.6 copy-start.48
  406.5 4.6 copy-start.49
  412.9 10.6 %copy-start.34 = (f32[128]{0:T(128)S(1)}, f32[128]{0:T(128)}, u32[]{:S(2)}) copy-start(f32[128]{0:T(128)} %param.24) | copy-start | bytes 1540
  413.6 9.8 %all-to-all-start = ((f32[8,1,1536]{2,1,0:T(1,128)}), f32[8,1,1536]{2,1,0:T(1,128)S(1)}, u32[]{:S(2)}, u32[]{:S(2)}) async-start(f32[8,1,1536]{2,1,0:T(1,128)} %broadcast_in_dim.2), calls=%async_computation | async-start | bytes 98304 | tf_op jit(solution)/shard_map/all_to_all | solution.py:39
  423.5 4.7 copy-start.75
  (34 other events, 138.7 us)
Sparse Core Ops, SparseCore 0:
  9.5 39.4 all-gather.11
  51.9 143.6 all-gather.13
  198.5 133.8 all-gather.15
where the time goes:
time: 492 us; the launch traced here: 487 us
  waiting for transfers between devices  168 us (34%)
  blocking collectives  126 us (26%)
  local copies, waits for them, and re-layouts  107 us (22%)
  other arithmetic  31.9 us (6%)
  matrix products  28 us (6%)
  between operations  14.7 us (3%)
  starting transfers between devices  12.5 us (3%)
    all_gather x1, waiting for transfers between devices, sent_together(): lax.all_gather(both, axis, axis=dim, tiled=True)  143 us
    all_gather x4, blocking collectives, all_in_one(): both, at, found = (lax.all_gather(jnp.concatenate(lines), axis), 0, {})  84 us
    all_to_all x1, blocking collectives, sum_at_owner(): lax.all_to_all(pieces, axis, split_axis=0, concat_axis=0, tiled=True)  41.7 us
    convert_element_type x40, local copies, waits for them, and re-layouts, prefix_by_axis(): part[k].astype(own.dtype)  38.4 us
    all_gather x1, waiting for transfers between devices, body(): lax.all_gather(tokens, 'tp', axis=0, tiled=True)  21.2 us
    mul x16, local copies, waits for them, and re-layouts, combine_branches(): latter[0][:, None, None] * earlier[1] + latter[1]  20 us
    dot_general x5, matrix products, body(): jnp.dot(normed, weight, preferred_element_type=jnp.float32)  11.6 us
  transfers between devices with their start and end apart: 6, of which 3 were waited for; matrix products, arithmetic and copies ran while one was open for 31% of the time, Pallas kernels for 0%

commit v1 on v0

--- a/solution.py
+++ b/solution.py
@@ -3,6 +3,7 @@
 from jax import lax
 from jax.sharding import Mesh
 from jax.sharding import PartitionSpec as P
+from jax.lax import all_to_all, axis_size
 
 DC = 1024
 HD = 64
@@ -184,6 +185,11 @@
     output_conv,
     output_heads,
 ):
+
+    def answer_seats_all(values):
+        left_arr = all_to_all(jnp.stack([values] * axis_size("tp")), "tp", 0, 0)
+        return jnp.concatenate(left_arr, 0)
+
     projections = (branch_value, branch_gate, query_weight, key_weight, value_weight, swish_weight)
     full_column_count = sent_together(
         (
@@ -198,7 +204,7 @@
         0,
         1,
     )
-    normed = normalize(lax.all_gather(tokens, "tp", axis=0, tiled=True), input_gain)
+    normed = normalize(answer_seats_all(tokens), input_gain)
     packed = input_mix(
         tuple(
             (

time: 492 us -> 458 us (0.931)
  waiting for transfers between devices: 168 us -> 127 us
    all_gather x1, waiting for transfers between devices: 143 us -> 98.5 us  [sent_together(): lax.all_gather(both, axis, axis=dim, tiled=True)]
    all_to_all x0 -> x1, waiting for transfers between devices: none -> 26.1 us  [answer_seats_all(): left_arr = all_to_all(jnp.stack([values] * axis_size('tp')), 'tp', 0, 0)]
    all_gather x1 -> x0, waiting for transfers between devices: 21.2 us -> none  [body(): lax.all_gather(tokens, 'tp', axis=0, tiled=True)]
  transfers between devices with their start and end apart: 6 -> 6, of which waited for: 3 -> 3; matrix products, arithmetic and copies ran while one was open for 31% -> 32% of each run, Pallas kernels for 0% -> 0%
where the time goes in v1:
time: 458 us; the launch traced here: 453 us
  waiting for transfers between devices  127 us (28%)
  blocking collectives  126 us (28%)
  local copies, waits for them, and re-layouts  108 us (24%)
  other arithmetic  31.1 us (7%)
  matrix products  28.9 us (6%)
  starting transfers between devices  16.8 us (4%)
  between operations  15 us (3%)
    all_gather x1, waiting for transfers between devices, sent_together(): lax.all_gather(both, axis, axis=dim, tiled=True)  98.5 us
    all_gather x4, blocking collectives, all_in_one(): both, at, found = (lax.all_gather(jnp.concatenate(lines), axis), 0, {})  84.4 us
    all_to_all x1, blocking collectives, sum_at_owner(): lax.all_to_all(pieces, axis, split_axis=0, concat_axis=0, tiled=True)  41.7 us
    convert_element_type x40, local copies, waits for them, and re-layouts, prefix_by_axis(): part[k].astype(own.dtype)  38.4 us
    all_to_all x1, waiting for transfers between devices, answer_seats_all(): left_arr = all_to_all(jnp.stack([values] * axis_size('tp')), 'tp', 0, 0)  26.1 us
    mul x16, local copies, waits for them, and re-layouts, combine_branches(): latter[0][:, None, None] * earlier[1] + latter[1]  19.9 us
    dot_general x5, matrix products, body(): jnp.dot(normed, weight, preferred_element_type=jnp.float32)  12.5 us
    reshape x6, local copies, waits for them, and re-layouts, split_heads(): return matrix.astype(jnp.float32).reshape(blocks, BLOCK, local_heads, HD)  9.85 us
  transfers between devices with their start and end apart: 6, of which 3 were waited for; matrix products, arithmetic and copies ran while one was open for 32% of the time, Pallas kernels for 0%

profile of v1, /device:TPU:32, one launch (start us, length us, event | category | flops | bytes accessed | tf_op | source)
XLA Modules:
  0.0 452.7 jit_solution(3704460201258676728)
XLA Ops:
  11.4 3.0 stack.6
  14.4 4.4 all-to-all-start
  19.8 1.8 reduce-window.6
  31.2 26.1 %all-to-all-done = bf16[8,96,2048]{2,1,0:T(8,128)(2,1)S(1)} async-done(((bf16[8,96,2048]{2,1,0:T(8,128)(2,1)}), bf16[8,96,2048]{2,1,0:T(8,128)(2,1)S(1)}, u32[]{:S(2)}, u32[]{:S(2)}) %all-to-all-start) | async-done | bytes 3145760 | tf_op jit(solution)/shard_map/all_to_all | solution.py:190
  58.1 2.6 fusion.1
  60.7 98.5 %all-gather.11.cloned.1.call-done = bf16[2048,768]{1,0:T(8,128)(2,1)} async-done(((bf16[32,768]{1,0:T(8,128)(2,1)}), bf16[2048,768]{1,0:T(8,128)(2,1)}) %all-gather.11.cloned.1.call-update) | async-done | bytes 3145744 | tf_op jit(solution)/shard_map/all_gather | solution.py:22
  159.2 3.0 convolution_convert_fusion.3
  164.4 2.8 fusion.28
  167.2 1.9 copy.305
  169.1 2.0 reshape.1754
  171.2 2.0 broadcast_multiply_fusion.2
  175.1 1.5 copy.317
  176.7 1.5 copy.319
  178.2 1.5 copy.318
  180.4 1.5 copy.348
  181.9 1.5 copy.350
  183.5 1.5 copy.349
  186.6 12.0 %all-gather.4 = bf16[4,129,64]{1,2,0:T(8,128)(2,1)S(1)} all-gather(bf16[1,129,64]{1,2,0:T(8,128)(2,1)S(1)} %get-tuple-element.78), channel_id=2, replica_groups=mesh['sp_0'=16,'sp_1'=4,'tp'=8] {'sp_1'}, dimensions={0}, use_global_device_ids=true | all-gather | bytes 82560 | tf_op jit(solution)/shard_map/all_gather | solution.py:70
  200.6 12.0 %all-gather.6 = bf16[4,129,64]{1,2,0:T(8,128)(2,1)S(1)} all-gather(bf16[1,129,64]{1,2,0:T(8,128)(2,1)S(1)} %get-tuple-element.79), channel_id=4, replica_groups=mesh['sp_0'=16,'sp_1'=4,'tp'=8] {'sp_1'}, dimensions={0}, use_global_device_ids=true | all-gather | bytes 82560 | tf_op jit(solution)/shard_map/all_gather | solution.py:70
  215.2 1.3 mul.1870
  224.1 1.3 mul.1880
  225.4 1.3 copy.352
  228.3 29.0 %all-gather.7 = bf16[16,129,64]{1,2,0:T(8,128)(2,1)S(1)} all-gather(bf16[1,129,64]{1,2,0:T(8,128)(2,1)S(1)} %maximum_bitcast_fusion.1), channel_id=5, replica_groups=mesh['sp_0'=16,'sp_1'=4,'tp'=8] {'sp_0'}, dimensions={0}, use_global_device_ids=true | all-gather | bytes 280704 | tf_op jit(solution)/shard_map/all_gather | solution.py:70
  262.5 1.3 mul.1769
  271.2 1.3 mul.1779
  275.3 31.4 %all-gather.5 = bf16[16,129,64]{1,2,0:T(8,128)(2,1)S(1)} all-gather(bf16[1,129,64]{1,2,0:T(8,128)(2,1)S(1)} %maximum_bitcast_fusion), channel_id=3, replica_groups=mesh['sp_0'=16,'sp_1'=4,'tp'=8] {'sp_0'}, dimensions={0}, use_global_device_ids=true | all-gather | bytes 280704 | tf_op jit(solution)/shard_map/all_gather | solution.py:70
  310.7 2.7 convolution_convert_fusion.2
  313.4 1.9 reshape.1862
  315.3 1.9 copy.306
  317.2 1.5 copy.339
  318.6 1.5 copy.341
  320.1 1.5 copy.340
  321.6 1.5 copy.342
  323.1 1.5 copy.370
  324.6 1.5 copy.372
  326.0 1.5 copy.371
  327.5 1.5 copy.373
  329.0 2.0 fusion.40
  331.0 2.0 fusion.26
  333.9 1.9 collective-permute-start
  335.8 6.2 %collective-permute-start.1 = (bf16[15,128]{1,0:T(8,128)(2,1)}, bf16[15,128]{1,0:T(8,128)(2,1)}, u32[]{:S(2)}, u32[]{:S(2)}) collective-permute-start(bf16[15,128]{1,0:T(8,128)(2,1)} %get-tuple-element.69), channel_id=1, source_target_pairs={{8,0},{16,8},{24,16},{32,24},{40,32},{48,40},{56,48},{64,56},{72,6... | collective-permute-start | bytes 11528 | tf_op jit(solution)/shard_map/ppermute | solution.py:33
  376.5 1.5 fusion.159
  378.7 4.2 all-to-all-start.1
  385.7 2.7 all-to-all-done.1
  388.5 4.7 %fusion.37 = f32[768,2048]{1,0:T(8,128)} fusion(bf16[2048,256]{1,0:T(8,128)(2,1)} %all-gather.13.cloned.1.call-done, f32[768,128]{1,0:T(8,128)S(1)} %get-tuple-element.26, f32[128]{0:T(128)S(1)} %copy-done.37, f32[768]{0:T(1024)S(1)} %get-tuple-element.112, f32[768]{0:T(1024)S(1)} %get-tuple-element.111), kind=kOutput, calls=%fused_computation.40 | convolution fusion | flops 403439616 | bytes 7215616 | tf_op jit(solution)/shard_map/dot_general | solution.py:288
  393.2 7.7 %add_convert_fusion = bf16[768,2048]{1,0:T(8,128)(2,1)S(1)} fusion(f32[768,2048]{1,0:T(8,128)} %fusion.37, bf16[2048,256]{1,0:T(8,128)(2,1)} %all-gather.13.cloned.1.call-done, bf16[768,2048]{1,0:T(8,128)(2,1)} %fusion.1, bf16[2048,768]{1,0:T(8,128)(2,1)} %all-gather.11.cloned.1.call-done, f32[768,128]{1,0:T(8,128)S(1)} %copy.379, ...), kind=kOutput, calls=%fused_computation.3 | convolution fusion | flops 809533440 | bytes 14811648 | tf_op jit(solution)/shard_map/dot_general | solution.py:290
  400.9 41.7 %all_to_all.16 = bf16[8,96,2048]{2,1,0:T(8,128)(2,1)} all-to-all(bf16[8,96,2048]{2,1,0:T(8,128)(2,1)S(1)} %bitcast.528), channel_id=1, replica_groups=mesh['sp_0'=16,'sp_1'=4,'tp'=8] {'tp'}, dimensions={0} | all-to-all | bytes 6291456 | tf_op jit(solution)/shard_map/all_to_all | solution.py:120
  442.6 3.3 reduce_sum.72
  (310 shorter events, 93.1 us)
Async XLA Ops:
  6.5 152.7 %all-gather.11.cloned.1.call-start = ((), (), s32[]{:S(2)}) async-start(), calls=%async_computation.3 | async-start | bytes 3194880 | tf_op jit(solution)/shard_map/all_gather | solution.py:22
  14.4 5.3 %copy-start.30 = (f32[2,768]{1,0:T(2,128)S(1)}, f32[2,768]{1,0:T(2,128)}, u32[]{:S(2)}) copy-start(f32[2,768]{1,0:T(2,128)} %param.25) | copy-start | bytes 18436
  14.4 14.9 %copy-start.25 = (f32[31,128]{1,0:T(8,128)S(1)}, f32[31,128]{1,0:T(8,128)}, u32[]{:S(2)}) copy-start(f32[31,128]{1,0:T(8,128)} %param.23) | copy-start | bytes 47620
  14.4 42.8 %all-to-all-start = ((bf16[8,96,2048]{2,1,0:T(8,128)(2,1)}), bf16[8,96,2048]{2,1,0:T(8,128)(2,1)S(1)}, u32[]{:S(2)}, u32[]{:S(2)}) async-start(bf16[8,96,2048]{2,1,0:T(8,128)(2,1)} %stack.6), calls=%async_computation | async-start | bytes 6291456 | tf_op jit(solution)/shard_map/all_to_all | solution.py:190
  18.9 39.2 %copy-start.26 = (f32[2048]{0:T(1024)S(1)}, f32[2048]{0:T(1024)}, u32[]{:S(2)}) copy-start(f32[2048]{0:T(1024)} %param.16) | copy-start | bytes 24580
  18.9 369.6 %all-gather.13.cloned.1.call-start = ((), (), s32[]{:S(2)}) async-start(), calls=%async_computation.4 | async-start | bytes 1064960 | tf_op jit(solution)/shard_map/all_gather | solution.py:104
  22.5 38.2 %copy-start.34 = (f32[2]{0:T(128)}, f32[2]{0:T(128)S(1)}, u32[]{:S(2)}) copy-start(f32[2]{0:T(128)S(1)} %get-tuple-element.7) | copy-start | bytes 28
  22.5 38.2 %copy-start.35 = (f32[2]{0:T(128)}, f32[2]{0:T(128)S(1)}, u32[]{:S(2)}) copy-start(f32[2]{0:T(128)S(1)} %get-tuple-element.8) | copy-start | bytes 28
  25.2 35.4 %copy-start.33 = (f32[2]{0:T(128)}, f32[2]{0:T(128)S(1)}, u32[]{:S(2)}) copy-start(f32[2]{0:T(128)S(1)} %get-tuple-element.156) | copy-start | bytes 28
  60.6 103.7 %copy-start = (bf16[768,2048]{1,0:T(8,128)(2,1)S(1)}, bf16[768,2048]{1,0:T(8,128)(2,1)}, u32[]{:S(2)}) copy-start(bf16[768,2048]{1,0:T(8,128)(2,1)} %fusion.1) | copy-start | bytes 9437188
  164.4 8.8 %copy-start.1 = (bf16[3,256,2,64]{1,3,2,0:T(8,128)(2,1)}, bf16[3,256,2,64]{1,3,2,0:T(8,128)(2,1)S(1)}, u32[]{:S(2)}) copy-start(bf16[3,256,2,64]{1,3,2,0:T(8,128)(2,1)S(1)} %copy.311) | copy-start | bytes 589828
  164.4 6.8 %copy-start.24 = (f32[3,256,2]{1,0,2:T(4,128)S(1)}, f32[3,256,2]{1,0,2:T(4,128)}, u32[]{:S(2)}) copy-start(f32[3,256,2]{1,0,2:T(4,128)} %copy.345) | copy-start | bytes 18436
  198.7 59.3 %copy-start.20 = (bf16[4,64]{1,0:T(4,128)(2,1)}, bf16[4,64]{1,0:T(4,128)(2,1)S(1)}, u32[]{:S(2)}) copy-start(bf16[4,64]{1,0:T(4,128)(2,1)S(1)} %slice_reduce_fusion.1) | copy-start | bytes 1540
  212.7 94.8 %copy-start.22 = (bf16[4,64]{1,0:T(4,128)(2,1)}, bf16[4,64]{1,0:T(4,128)(2,1)S(1)}, u32[]{:S(2)}) copy-start(bf16[4,64]{1,0:T(4,128)(2,1)S(1)} %slice_reduce_fusion) | copy-start | bytes 1540
  333.1 9.0 %copy-start.16 = (bf16[768,128]{1,0:T(8,128)(2,1)}, bf16[768,128]{1,0:T(8,128)(2,1)S(1)}, u32[]{:S(2)}) copy-start(bf16[768,128]{1,0:T(8,128)(2,1)S(1)} %fusion.26) | copy-start | bytes 589828
  333.1 35.6 %copy-start.18 = (f32[1,128,64]{1,2,0:T(8,128)S(1)}, f32[1,128,64]{1,2,0:T(8,128)}, u32[]{:S(2)}) copy-start(f32[1,128,64]{1,2,0:T(8,128)} %get-tuple-element.45) | copy-start | bytes 98308
  333.1 35.7 %copy-start.23 = (bf16[4,64]{1,0:T(4,128)(2,1)S(1)}, bf16[4,64]{1,0:T(4,128)(2,1)}, u32[]{:S(2)}) copy-start(bf16[4,64]{1,0:T(4,128)(2,1)} %copy-done.22) | copy-start | bytes 1540
  333.1 35.7 %copy-start.46 = (f32[2]{0:T(128)S(1)}, f32[2]{0:T(128)}, u32[]{:S(2)}) copy-start(f32[2]{0:T(128)} %get-tuple-element.23) | copy-start | bytes 28
  333.1 35.8 %copy-start.21 = (bf16[4,64]{1,0:T(4,128)(2,1)S(1)}, bf16[4,64]{1,0:T(4,128)(2,1)}, u32[]{:S(2)}) copy-start(bf16[4,64]{1,0:T(4,128)(2,1)} %copy-done.20) | copy-start | bytes 1540
  333.1 35.8 %copy-start.45 = (f32[2]{0:T(128)S(1)}, f32[2]{0:T(128)}, u32[]{:S(2)}) copy-start(f32[2]{0:T(128)} %get-tuple-element.15) | copy-start | bytes 28
  333.1 35.8 %copy-start.10 = (f32[1,128,64]{2,1,0:T(8,128)S(1)}, f32[1,128,64]{2,1,0:T(8,128)}, u32[]{:S(2)}) copy-start(f32[1,128,64]{2,1,0:T(8,128)} %copy.339) | copy-start | bytes 98308
  333.1 35.8 %copy-start.11 = (f32[1,128,64]{2,1,0:T(8,128)S(1)}, f32[1,128,64]{2,1,0:T(8,128)}, u32[]{:S(2)}) copy-start(f32[1,128,64]{2,1,0:T(8,128)} %copy.341) | copy-start | bytes 98308
  333.1 35.8 %copy-start.12 = (f32[1,128,64]{2,1,0:T(8,128)S(1)}, f32[1,128,64]{2,1,0:T(8,128)}, u32[]{:S(2)}) copy-start(f32[1,128,64]{2,1,0:T(8,128)} %copy.340) | copy-start | bytes 98308
  333.1 35.8 %copy-start.13 = (f32[1,128,64]{2,1,0:T(8,128)S(1)}, f32[1,128,64]{2,1,0:T(8,128)}, u32[]{:S(2)}) copy-start(f32[1,128,64]{2,1,0:T(8,128)} %copy.342) | copy-start | bytes 98308
  333.2 35.8 %copy-start.32 = (f32[2]{0:T(128)S(1)}, f32[2]{0:T(128)}, u32[]{:S(2)}) copy-start(f32[2]{0:T(128)} %copy-done.31) | copy-start | bytes 28
  333.2 35.8 %copy-start.36 = (f32[2]{0:T(128)S(1)}, f32[2]{0:T(128)}, u32[]{:S(2)}) copy-start(f32[2]{0:T(128)} %copy-done.35) | copy-start | bytes 28
  333.2 35.8 %copy-start.38 = (f32[2]{0:T(128)S(1)}, f32[2]{0:T(128)}, u32[]{:S(2)}) copy-start(f32[2]{0:T(128)} %get-tuple-element.147) | copy-start | bytes 28
  333.2 35.8 %copy-start.39 = (f32[2]{0:T(128)S(1)}, f32[2]{0:T(128)}, u32[]{:S(2)}) copy-start(f32[2]{0:T(128)} %get-tuple-element.114) | copy-start | bytes 28
  333.2 35.8 %copy-start.40 = (f32[2]{0:T(128)S(1)}, f32[2]{0:T(128)}, u32[]{:S(2)}) copy-start(f32[2]{0:T(128)} %get-tuple-element.115) | copy-start | bytes 28
  333.2 35.8 %copy-start.41 = (f32[2]{0:T(128)S(1)}, f32[2]{0:T(128)}, u32[]{:S(2)}) copy-start(f32[2]{0:T(128)} %get-tuple-element.116) | copy-start | bytes 28
  333.2 35.8 %copy-start.42 = (f32[2]{0:T(128)S(1)}, f32[2]{0:T(128)}, u32[]{:S(2)}) copy-start(f32[2]{0:T(128)} %get-tuple-element.117) | copy-start | bytes 28
  333.2 35.8 %copy-start.43 = (f32[2]{0:T(128)S(1)}, f32[2]{0:T(128)}, u32[]{:S(2)}) copy-start(f32[2]{0:T(128)} %get-tuple-element.118) | copy-start | bytes 28
  333.2 37.0 %copy-start.6 = (f32[1,128,64]{2,1,0:T(8,128)S(1)}, f32[1,128,64]{2,1,0:T(8,128)}, u32[]{:S(2)}) copy-start(f32[1,128,64]{2,1,0:T(8,128)} %copy.370) | copy-start | bytes 98308
  333.2 37.0 %copy-start.7 = (f32[1,128,64]{2,1,0:T(8,128)S(1)}, f32[1,128,64]{2,1,0:T(8,128)}, u32[]{:S(2)}) copy-start(f32[1,128,64]{2,1,0:T(8,128)} %copy.372) | copy-start | bytes 98308
  333.3 37.0 %copy-start.8 = (f32[1,128,64]{2,1,0:T(8,128)S(1)}, f32[1,128,64]{2,1,0:T(8,128)}, u32[]{:S(2)}) copy-start(f32[1,128,64]{2,1,0:T(8,128)} %copy.371) | copy-start | bytes 98308
  333.3 37.0 %copy-start.9 = (f32[1,128,64]{2,1,0:T(8,128)S(1)}, f32[1,128,64]{2,1,0:T(8,128)}, u32[]{:S(2)}) copy-start(f32[1,128,64]{2,1,0:T(8,128)} %copy.373) | copy-start | bytes 98308
  333.9 41.5 %collective-permute-start = (bf16[15,128]{1,0:T(8,128)(2,1)}, bf16[15,128]{1,0:T(8,128)(2,1)}, u32[]{:S(2)}, u32[]{:S(2)}) collective-permute-start(bf16[15,128]{1,0:T(8,128)(2,1)} %get-tuple-element.68), channel_id=1, source_target_pairs={{0,8},{8,16},{16,24},{24,32},{32,40},{40,48},{48,56},{56,64},{64,7... | collective-permute-start | bytes 11528 | tf_op jit(solution)/shard_map/ppermute | solution.py:32
  335.8 39.6 %collective-permute-start.1 = (bf16[15,128]{1,0:T(8,128)(2,1)}, bf16[15,128]{1,0:T(8,128)(2,1)}, u32[]{:S(2)}, u32[]{:S(2)}) collective-permute-start(bf16[15,128]{1,0:T(8,128)(2,1)} %get-tuple-element.69), channel_id=1, source_target_pairs={{8,0},{16,8},{24,16},{32,24},{40,32},{48,40},{56,48},{64,56},{72,6... | collective-permute-start | bytes 11528 | tf_op jit(solution)/shard_map/ppermute | solution.py:33
  348.0 24.6 %copy-start.3 = (bf16[3,256,2,64]{1,3,2,0:T(8,128)(2,1)S(1)}, bf16[3,256,2,64]{1,3,2,0:T(8,128)(2,1)}, u32[]{:S(2)}) copy-start(bf16[3,256,2,64]{1,3,2,0:T(8,128)(2,1)} %copy.306) | copy-start | bytes 589828
  360.9 13.6 %copy-start.2 = (bf16[3,256,2,64]{1,3,2,0:T(8,128)(2,1)S(1)}, bf16[3,256,2,64]{1,3,2,0:T(8,128)(2,1)}, u32[]{:S(2)}) copy-start(bf16[3,256,2,64]{1,3,2,0:T(8,128)(2,1)} %copy-done.1) | copy-start | bytes 589828
  371.5 4.7 %copy-start.47 = (f32[128]{0:T(128)S(1)}, f32[128]{0:T(128)}, u32[]{:S(2)}) copy-start(f32[128]{0:T(128)} %get-tuple-element.99) | copy-start | bytes 1540
  371.5 4.7 %copy-start.48 = (f32[128]{0:T(128)S(1)}, f32[128]{0:T(128)}, u32[]{:S(2)}) copy-start(f32[128]{0:T(128)} %get-tuple-element.100) | copy-start | bytes 1540
  371.5 4.7 %copy-start.49 = (f32[128]{0:T(128)S(1)}, f32[128]{0:T(128)}, u32[]{:S(2)}) copy-start(f32[128]{0:T(128)} %get-tuple-element.101) | copy-start | bytes 1540
  371.5 4.7 %copy-start.50 = (f32[128]{0:T(128)S(1)}, f32[128]{0:T(128)}, u32[]{:S(2)}) copy-start(f32[128]{0:T(128)} %get-tuple-element.102) | copy-start | bytes 1540
  371.5 4.7 %copy-start.51 = (f32[128]{0:T(128)S(1)}, f32[128]{0:T(128)}, u32[]{:S(2)}) copy-start(f32[128]{0:T(128)} %get-tuple-element.103) | copy-start | bytes 1540
  378.0 10.5 %copy-start.37 = (f32[128]{0:T(128)S(1)}, f32[128]{0:T(128)}, u32[]{:S(2)}) copy-start(f32[128]{0:T(128)} %param.24) | copy-start | bytes 1540
  378.7 9.7 %all-to-all-start.1 = ((f32[8,1,1536]{2,1,0:T(1,128)}), f32[8,1,1536]{2,1,0:T(1,128)S(1)}, u32[]{:S(2)}, u32[]{:S(2)}) async-start(f32[8,1,1536]{2,1,0:T(1,128)} %broadcast_in_dim.2), calls=%async_computation.1 | async-start | bytes 98304 | tf_op jit(solution)/shard_map/all_to_all | solution.py:40
  388.5 4.7 %copy-start.78 = (f32[128]{0:T(128)S(1)}, f32[128]{0:T(128)}, u32[]{:S(2)}) copy-start(f32[128]{0:T(128)} %param.27) | copy-start | bytes 1540
  (37 other events, 152.5 us)
Sparse Core Ops, SparseCore 0:
  11.5 147.6 all-gather.10
  162.1 133.9 all-gather.12
